TPU v7x, 32 devices: a whole 2x2x4 slice. The times are simulated.
32 devices in a mesh: fs: 16 (over z, y, x), tp: 2 (over core).
Axes of the slice: x: 2, y: 2, z: 4, core: 2. Of those that a mesh axis runs over, the one named last changes fastest.
Arguments:
- inputs: bfloat16 [8192, 2048], P('fs', 'tp'), may hold values from -6 to 6
- value_cotangent: bfloat16 [8192, 2048], P('fs', 'tp'), may hold values from -6 to 6
- first_map: bfloat16 [8192, 2048], P('fs', 'tp'), may hold values from -6 to 6
- second_map: bfloat16 [8192, 2048], P('fs', 'tp'), may hold values from -6 to 6
- lambdas: float32 [16], P('tp'), may hold values from 0.3 to 0.8
- head_gain: float32 [128], replicated, may hold values from 0.1 to 1.9
- output_cotangent: bfloat16 [8192, 2048], P('fs', 'tp'), may hold values from -6 to 6
- value_factor: bfloat16 [2048, 256], replicated, may hold values from -0.125 to 0.125
- output_factor: bfloat16 [2048, 256], replicated, may hold values from -0.125 to 0.125
- value_weight: float32 [2048, 2048], P('fs', 'tp'), may hold values from -0.125 to 0.125
- output_weight: float32 [2048, 2048], P('tp', 'fs'), may hold values from -0.125 to 0.125
- value_moment: float32 [256, 2048], P('fs', 'tp'), may hold values from -6 to 6
- value_second: float32 [256, 2048], P('fs', 'tp'), may hold values from 0.25 to 4
- output_moment: float32 [256, 2048], P('fs', 'tp'), may hold values from -6 to 6
- output_second: float32 [256, 2048], P('fs', 'tp'), may hold values from 0.25 to 4
Outputs:
- value_master: float32 [2048, 2048], P('fs', 'tp')
- output_master: float32 [2048, 2048], P('tp', 'fs')
- value_moment_new: float32 [256, 2048], P('fs', 'tp')
- value_second_new: float32 [256, 2048], P('fs', 'tp')
- output_moment_new: float32 [256, 2048], P('fs', 'tp')
- output_second_new: float32 [256, 2048], P('fs', 'tp')
- value_copy: bfloat16 [2048, 2048], P(None, 'tp')
- output_copy: bfloat16 [2048, 2048], P('tp')
All inputs are finite; a program needn't handle non-finite values.
Results may differ from a plain program's by a relative error of at most 0.0027.
Values may be sent and summed in bfloat16 or wider, within the bound.
A program may use at most 64 MiB of HBM per device.

v0:
```python
import math
import jax
import jax.numpy as jnp
from jax import lax
from jax.sharding import PartitionSpec as P


def contract_rows(left, right, precise):
    if precise:
        return lax.dot_general(
            left,
            right,
            (((0,), (0,)), ((), ())),
            precision=lax.Precision.HIGHEST,
            preferred_element_type=jnp.float32,
        )
    return lax.dot_general(
        left, right, (((0,), (0,)), ((), ())), preferred_element_type=jnp.float32
    )


def local(
    inputs,
    value_cotangent,
    first_map,
    second_map,
    lambdas,
    head_gain,
    output_cotangent,
    value_factor,
    output_factor,
    value_weight,
    output_weight,
    value_moment,
    value_second,
    output_moment,
    output_second,
):
    tok_rows = inputs.shape[0]
    local_heads = lambdas.shape[0]
    head_width = head_gain.shape[0]
    head_cols = local_heads * head_width
    first = first_map.astype(jnp.float32).reshape(tok_rows, local_heads, head_width)
    second = second_map.astype(jnp.float32).reshape(tok_rows, local_heads, head_width)
    difference = first - lambdas[None, :, None] * second
    normed = (
        difference
        * lax.rsqrt(jnp.mean(difference * difference, axis=-1, keepdims=True) + 1e-06)
        * head_gain
    )
    heads_out = normed.reshape(tok_rows, head_cols).astype(jnp.bfloat16)
    full_inputs, full_cotangent = (
        lax.all_gather(inputs, "tp", axis=1, tiled=True),
        lax.all_gather(output_cotangent, "tp", axis=1, tiled=True),
    )
    token_scale = 1.0 / math.sqrt(tok_rows * lax.axis_size("fs"))
    fs_index = lax.axis_index("fs")
    width_rows = value_weight.shape[0]
    value_rows = lax.dynamic_slice_in_dim(
        value_factor, fs_index * width_rows, width_rows, 0
    ).astype(jnp.float32)
    output_rows = lax.dynamic_slice_in_dim(
        output_factor, fs_index * width_rows, width_rows, 0
    ).astype(jnp.float32)
    grad_value = contract_rows(full_inputs, value_cotangent, False) * token_scale
    grad_output = contract_rows(full_cotangent, heads_out, False) * token_scale
    partial_value = jnp.concatenate(
        [
            contract_rows(value_factor.astype(jnp.float32), grad_value, True),
            contract_rows(output_factor.astype(jnp.float32), grad_output, True),
        ],
        axis=1,
    )
    own_rows = lax.psum_scatter(partial_value, "fs", scatter_dimension=0, tiled=True)
    moments = jnp.concatenate([value_moment, output_moment], axis=1)
    seconds = jnp.concatenate([value_second, output_second], axis=1)
    moment_new = 0.8 * moments + 0.2 * own_rows
    second_new = 0.95 * seconds + 0.05 * own_rows * own_rows
    direction = moment_new / (jnp.sqrt(second_new) + 1e-08)
    full_direction = lax.all_gather(direction, "fs", axis=0, tiled=True)
    step_value = jnp.dot(
        value_rows,
        full_direction[:, :head_cols],
        precision=lax.Precision.HIGHEST,
        preferred_element_type=jnp.float32,
    )
    step_output = jnp.dot(
        output_rows,
        full_direction[:, head_cols:],
        precision=lax.Precision.HIGHEST,
        preferred_element_type=jnp.float32,
    )
    value_master = value_weight - 0.05 * step_value
    output_master = output_weight - 0.05 * step_output.T
    value_copy, output_copy = (
        lax.all_gather(value_master.astype(jnp.bfloat16), "fs", axis=0, tiled=True),
        lax.all_gather(output_master.astype(jnp.bfloat16), "fs", axis=1, tiled=True),
    )
    return (
        value_master,
        output_master,
        moment_new[:, :head_cols],
        second_new[:, :head_cols],
        moment_new[:, head_cols:],
        second_new[:, head_cols:],
        value_copy,
        output_copy,
    )


def solution(mesh):
    in_specs = (
        P("fs", "tp"),
        P("fs", "tp"),
        P("fs", "tp"),
        P("fs", "tp"),
        P("tp"),
        P(),
        P("fs", "tp"),
        P(),
        P(),
        P("fs", "tp"),
        P("tp", "fs"),
        P("fs", "tp"),
        P("fs", "tp"),
        P("fs", "tp"),
        P("fs", "tp"),
    )
    out_specs = (
        P("fs", "tp"),
        P("tp", "fs"),
        P("fs", "tp"),
        P("fs", "tp"),
        P("fs", "tp"),
        P("fs", "tp"),
        P(None, "tp"),
        P("tp", None),
    )
    return jax.shard_map(local, mesh=mesh, in_specs=in_specs, out_specs=out_specs, check_vma=False)
```

profile of v0, /device:TPU:0, one launch (start us, length us, event | category | flops | bytes accessed | tf_op | source)
XLA Modules:
  0.0 374.0 jit_solution(844891537116236253)
XLA Ops:
  7.2 0.7 all-gather.8.cloned.1.call-update
  8.0 0.7 all-gather.6.cloned.1.call-update
  9.5 0.7 copy-done.2
  11.4 0.6 multiply_reduce_fusion
  12.4 10.5 %all-gather.8.cloned.1.call-done = bf16[512,2048]{1,0:T(8,128)(2,1)} async-done(((bf16[512,1024]{1,0:T(8,128)(2,1)}), bf16[512,2048]{1,0:T(8,128)(2,1)}) %all-gather.8.cloned.1.call-update) | async-done | bytes 2097168 | tf_op jit(solution)/shard_map/all_gather | solution.py:54
  22.9 0.6 mul.105
  23.5 1.0 copy-done.5
  24.5 2.8 fusion.18
  27.3 4.0 %fusion.13 = f32[256,1024]{0,1:T(8,128)S(1)} fusion(bf16[2048,256]{1,0:T(8,128)(2,1)S(1)} %copy-done.8, f32[1024,2048]{1,0:T(8,128)S(1)} %fusion.18), kind=kOutput, calls=%fused_computation.18 | convolution fusion | flops 6444548096 | bytes 10485760 | tf_op jit(solution)/shard_map/dot_general | solution.py:10
  31.4 4.8 %all-gather.6.cloned.1.call-done = bf16[512,2048]{1,0:T(8,128)(2,1)} async-done(((bf16[512,1024]{1,0:T(8,128)(2,1)}), bf16[512,2048]{1,0:T(8,128)(2,1)}) %all-gather.6.cloned.1.call-update) | async-done | bytes 2097168 | tf_op jit(solution)/shard_map/all_gather | solution.py:53
  36.2 4.0 %fusion.38 = f32[2048,1024]{1,0:T(8,128)S(1)} fusion(bf16[512,2048]{1,0:T(8,128)(2,1)} %all-gather.6.cloned.1.call-done, bf16[512,1024]{1,0:T(8,128)(2,1)S(1)} %copy-done), kind=kOutput, calls=%fused_computation.47 | convolution fusion | flops 2147483648 | bytes 11534336 | tf_op jit(solution)/shard_map/dot_general | solution.py:17
  40.2 6.9 %fusion.10 = f32[256,1024]{0,1:T(8,128)S(1)} fusion(bf16[2048,256]{1,0:T(8,128)(2,1)S(1)} %copy-done.7, f32[2048,1024]{1,0:T(8,128)S(1)} %fusion.38), kind=kOutput, calls=%fused_computation.17 | convolution fusion | flops 6444548096 | bytes 10485760 | tf_op jit(solution)/shard_map/dot_general | solution.py:10
  47.3 1.8 copy.49
  49.3 82.7 %reduce-scatter.4.cloned.1.call-done = f32[16,2048]{1,0:T(8,128)} async-done(((f32[256,2048]{1,0:T(8,128)}), f32[16,2048]{1,0:T(8,128)}) %reduce-scatter.4.cloned.1.call-update) | async-done | bytes 131088 | tf_op jit(solution)/shard_map/reduce_scatter | solution.py:74
  132.0 1.6 add_divide_fusion
  133.7 58.5 %all-gather.10.cloned.1.call-done = f32[256,2048]{1,0:T(8,128)} async-done(((f32[16,2048]{1,0:T(8,128)}), f32[256,2048]{1,0:T(8,128)}) %all-gather.10.cloned.1.call-update) | async-done | bytes 2097168 | tf_op jit(solution)/shard_map/all_gather | solution.py:80
  192.2 2.8 fusion.36
  195.1 2.7 fusion.37
  197.8 0.7 fusion.35
  198.5 0.7 fusion.34
  199.1 70.7 %all-gather.12.cloned.1.call-done = bf16[2048,1024]{1,0:T(8,128)(2,1)} async-done(((bf16[128,1024]{1,0:T(8,128)(2,1)}), bf16[2048,1024]{1,0:T(8,128)(2,1)}) %all-gather.12.cloned.1.call-update) | async-done | bytes 4194320 | tf_op jit(solution)/shard_map/all_gather | solution.py:96
  269.8 90.5 %all-gather.14.cloned.1.call-done = bf16[1024,2048]{1,0:T(8,128)(2,1)} async-done(((bf16[1024,128]{1,0:T(8,128)(2,1)}), bf16[1024,2048]{1,0:T(8,128)(2,1)}) %all-gather.14.cloned.1.call-update) | async-done | bytes 4194320 | tf_op jit(solution)/shard_map/all_gather | solution.py:97
  360.3 4.8 %copy.58 = bf16[2048,1024]{1,0:T(8,128)(2,1)} copy(bf16[2048,1024]{1,0:T(8,128)(2,1)} %all-gather.12.cloned.1.call-done) | data formatting | bytes 8388608
  365.1 2.0 copy.59
  (52 shorter events, 2.7 us)
Async XLA Ops:
  7.2 29.0 %copy-start = (bf16[512,1024]{1,0:T(8,128)(2,1)S(1)}, bf16[512,1024]{1,0:T(8,128)(2,1)}, u32[]{:S(2)}) copy-start(bf16[512,1024]{1,0:T(8,128)(2,1)} %param.16) | copy-start | bytes 3145732
  7.2 1.5 copy-start.3
  7.2 15.7 %all-gather.8.cloned.1.call-start = ((), (), s32[]{:S(2)}) async-start(), calls=%async_computation.2 | async-start | bytes 3145728 | tf_op jit(solution)/shard_map/all_gather | solution.py:54
  7.9 28.3 %all-gather.6.cloned.1.call-start = ((), (), s32[]{:S(2)}) async-start(), calls=%async_computation.1 | async-start | bytes 3145728 | tf_op jit(solution)/shard_map/all_gather | solution.py:53
  8.7 123.3 %reduce-scatter.4.cloned.1.call-start = ((), (), s32[]{:S(2)}) async-start(), calls=%async_computation.6 | async-start | bytes 2228224 | tf_op jit(solution)/shard_map/reduce_scatter | solution.py:74
  9.0 1.2 copy-start.2
  10.5 0.7 copy-start.15
  11.4 0.9 copy-start.16
  22.9 1.6 copy-start.5
  24.5 2.8 copy-start.8
  31.4 8.9 %copy-start.7 = (bf16[2048,256]{1,0:T(8,128)(2,1)S(1)}, bf16[2048,256]{1,0:T(8,128)(2,1)}, u32[]{:S(2)}) copy-start(bf16[2048,256]{1,0:T(8,128)(2,1)} %param.22) | copy-start | bytes 3145732
  49.1 82.9 %copy-start.11 = (f32[16,1024]{1,0:T(8,128)S(1)}, f32[16,1024]{1,0:T(8,128)}, u32[]{:S(2)}) copy-start(f32[16,1024]{1,0:T(8,128)} %param.29) | copy-start | bytes 196612
  49.1 82.9 %copy-start.12 = (f32[16,1024]{1,0:T(8,128)S(1)}, f32[16,1024]{1,0:T(8,128)}, u32[]{:S(2)}) copy-start(f32[16,1024]{1,0:T(8,128)} %param.27) | copy-start | bytes 196612
  49.1 82.9 %copy-start.13 = (f32[16,1024]{1,0:T(8,128)S(1)}, f32[16,1024]{1,0:T(8,128)}, u32[]{:S(2)}) copy-start(f32[16,1024]{1,0:T(8,128)} %param.28) | copy-start | bytes 196612
  49.1 82.9 %copy-start.14 = (f32[16,1024]{1,0:T(8,128)S(1)}, f32[16,1024]{1,0:T(8,128)}, u32[]{:S(2)}) copy-start(f32[16,1024]{1,0:T(8,128)} %param.26) | copy-start | bytes 196612
  49.2 143.0 %copy-start.9 = (f32[128,1024]{1,0:T(8,128)S(1)}, f32[128,1024]{1,0:T(8,128)}, u32[]{:S(2)}) copy-start(f32[128,1024]{1,0:T(8,128)} %param.24) | copy-start | bytes 1572868
  49.2 145.9 %copy-start.10 = (f32[1024,128]{1,0:T(8,128)S(1)}, f32[1024,128]{1,0:T(8,128)}, u32[]{:S(2)}) copy-start(f32[1024,128]{1,0:T(8,128)} %param.25) | copy-start | bytes 1572868
  49.2 143.0 %all-gather.10.cloned.1.call-start = ((), (), s32[]{:S(2)}) async-start(), calls=%async_computation.3 | async-start | bytes 2228224 | tf_op jit(solution)/shard_map/all_gather | solution.py:80
  133.7 136.1 %all-gather.12.cloned.1.call-start = ((), (), s32[]{:S(2)}) async-start(), calls=%async_computation.4 | async-start | bytes 4456448 | tf_op jit(solution)/shard_map/all_gather | solution.py:96
  192.2 2.9 copy-start.6
  195.0 165.3 %all-gather.14.cloned.1.call-start = ((), (), s32[]{:S(2)}) async-start(), calls=%async_computation.5 | async-start | bytes 4456448 | tf_op jit(solution)/shard_map/all_gather | solution.py:97
  360.3 4.8 %copy-start.4 = (bf16[1024,2048]{1,0:T(8,128)(2,1)S(1)}, bf16[1024,2048]{1,0:T(8,128)(2,1)}, u32[]{:S(2)}) copy-start(bf16[1024,2048]{1,0:T(8,128)(2,1)} %all-gather.14.cloned.1.call-done) | copy-start | bytes 12582916
  365.1 2.0 copy-start.1
Sparse Core Ops, SparseCore 0:
  9.5 13.2 all-gather.7
  24.4 11.7 all-gather.5
  49.3 82.6 reduce-scatter.3
  135.2 56.9 all-gather.9
  195.4 74.3 all-gather.11
  272.9 87.3 all-gather.13
where the time goes:
time: 374 us
  waiting for transfers between devices  319 us (85%)
  matrix products  23.3 us (6%)
  between operations  14.3 us (4%)
  local copies, waits for them, and re-layouts  13.8 us (4%)
    all_gather x1, waiting for transfers between devices, local(): lax.all_gather(output_master.astype(jnp.bfloat16), 'fs', axis=1, tiled=True)  90.5 us
    reduce_scatter x1, waiting for transfers between devices, local(): lax.psum_scatter(partial_value, 'fs', scatter_dimension=0, tiled=True)  82.7 us
    all_gather x1, waiting for transfers between devices, local(): lax.all_gather(value_master.astype(jnp.bfloat16), 'fs', axis=0, tiled=True)  70.7 us
    all_gather x1, waiting for transfers between devices, local(): full_direction = lax.all_gather(direction, 'fs', axis=0, tiled=True)  58.5 us
    unnamed x39, local copies, waits for them, and re-layouts  11.6 us
    dot_general x2, matrix products, contract_rows(): lax.dot_general(left, right, (((0,), (0,)), ((), ())), precision=lax.Prec...  10.9 us
    all_gather x1, waiting for transfers between devices, local(): lax.all_gather(output_cotangent, 'tp', axis=1, tiled=True)  10.5 us
  transfers between devices with their start and end apart: 6, of which 6 were waited for; matrix products, arithmetic and copies ran while one was open for 4% of the time, Pallas kernels for 0%

commit v1 on v0

--- a/solution.py
+++ b/solution.py
@@ -3,6 +3,12 @@
 import jax.numpy as jnp
 from jax import lax
 from jax.sharding import PartitionSpec as P
+
+
+def gather_blocks(x, mesh_axis, dim):
+    parts = lax.all_gather(x, mesh_axis, axis=0, tiled=False)
+    whole = jnp.concatenate(parts, axis=dim)
+    return whole
 
 
 def contract_rows(left, right, precise):
@@ -94,7 +100,7 @@
     output_master = output_weight - 0.05 * step_output.T
     value_copy, output_copy = (
         lax.all_gather(value_master.astype(jnp.bfloat16), "fs", axis=0, tiled=True),
-        lax.all_gather(output_master.astype(jnp.bfloat16), "fs", axis=1, tiled=True),
+        gather_blocks(output_master.astype(jnp.bfloat16), "fs", 1),
     )
     return (
         value_master,

time: 374 us -> 359 us (0.960)
  waiting for transfers between devices: 319 us -> 301 us
    all_gather x1, waiting for transfers between devices: 90.5 us -> 70.9 us  [gather_blocks(): parts = lax.all_gather(x, mesh_axis, axis=0, tiled=False)]
    reshape x0 -> x1, local copies, waits for them, and re-layouts: none -> 5.4 us  [gather_blocks(): whole = jnp.concatenate(parts, axis=dim)]
    unnamed x39 -> x36, local copies, waits for them, and re-layouts: 11.6 us -> 9.46 us
  transfers between devices with their start and end apart: 6 -> 6, of which waited for: 6 -> 6; matrix products, arithmetic and copies ran while one was open for 4% -> 5% of each run, Pallas kernels for 0% -> 0%
where the time goes in v1:
time: 359 us
  waiting for transfers between devices  301 us (84%)
  matrix products  23.3 us (6%)
  local copies, waits for them, and re-layouts  17.1 us (5%)
  between operations  14.3 us (4%)
    reduce_scatter x1, waiting for transfers between devices, local(): lax.psum_scatter(partial_value, 'fs', scatter_dimension=0, tiled=True)  82.7 us
    all_gather x1, waiting for transfers between devices, local(): lax.all_gather(value_master.astype(jnp.bfloat16), 'fs', axis=0, tiled=True)  72 us
    all_gather x1, waiting for transfers between devices, gather_blocks(): parts = lax.all_gather(x, mesh_axis, axis=0, tiled=False)  70.9 us
    all_gather x1, waiting for transfers between devices, local(): full_direction = lax.all_gather(direction, 'fs', axis=0, tiled=True)  58.5 us
    dot_general x2, matrix products, contract_rows(): lax.dot_general(left, right, (((0,), (0,)), ((), ())), precision=lax.Prec...  10.9 us
    all_gather x1, waiting for transfers between devices, local(): lax.all_gather(output_cotangent, 'tp', axis=1, tiled=True)  10.5 us
    unnamed x36, local copies, waits for them, and re-layouts  9.46 us
  transfers between devices with their start and end apart: 6, of which 6 were waited for; matrix products, arithmetic and copies ran while one was open for 5% of the time, Pallas kernels for 0%

profile of v1, /device:TPU:0, one launch (start us, length us, event | category | flops | bytes accessed | tf_op | source)
XLA Modules:
  0.0 359.0 jit_solution(16300867602004789932)
XLA Ops:
  7.2 0.7 all-gather.9.cloned.1.call-update
  8.0 0.7 all-gather.7.cloned.1.call-update
  9.5 0.7 copy-done.2
  11.4 0.6 multiply_reduce_fusion
  12.4 10.5 %all-gather.9.cloned.1.call-done = bf16[512,2048]{1,0:T(8,128)(2,1)} async-done(((bf16[512,1024]{1,0:T(8,128)(2,1)}), bf16[512,2048]{1,0:T(8,128)(2,1)}) %all-gather.9.cloned.1.call-update) | async-done | bytes 2097168 | tf_op jit(solution)/shard_map/all_gather | solution.py:60
  22.9 0.6 mul.105
  23.5 1.0 copy-done.4
  24.5 2.8 fusion.18
  27.3 4.0 %fusion.13 = f32[256,1024]{0,1:T(8,128)S(1)} fusion(bf16[2048,256]{1,0:T(8,128)(2,1)S(1)} %copy-done.6, f32[1024,2048]{1,0:T(8,128)S(1)} %fusion.18), kind=kOutput, calls=%fused_computation.19 | convolution fusion | flops 6444548096 | bytes 10485760 | tf_op jit(solution)/shard_map/dot_general | solution.py:16
  31.4 4.8 %all-gather.7.cloned.1.call-done = bf16[512,2048]{1,0:T(8,128)(2,1)} async-done(((bf16[512,1024]{1,0:T(8,128)(2,1)}), bf16[512,2048]{1,0:T(8,128)(2,1)}) %all-gather.7.cloned.1.call-update) | async-done | bytes 2097168 | tf_op jit(solution)/shard_map/all_gather | solution.py:59
  36.2 4.0 %fusion.38 = f32[2048,1024]{1,0:T(8,128)S(1)} fusion(bf16[512,2048]{1,0:T(8,128)(2,1)} %all-gather.7.cloned.1.call-done, bf16[512,1024]{1,0:T(8,128)(2,1)S(1)} %copy-done), kind=kOutput, calls=%fused_computation.48 | convolution fusion | flops 2147483648 | bytes 11534336 | tf_op jit(solution)/shard_map/dot_general | solution.py:23
  40.2 6.9 %fusion.10 = f32[256,1024]{0,1:T(8,128)S(1)} fusion(bf16[2048,256]{1,0:T(8,128)(2,1)S(1)} %copy-done.7, f32[2048,1024]{1,0:T(8,128)S(1)} %fusion.38), kind=kOutput, calls=%fused_computation.18 | convolution fusion | flops 6444548096 | bytes 10485760 | tf_op jit(solution)/shard_map/dot_general | solution.py:16
  47.3 1.8 copy.53
  49.3 82.7 %reduce-scatter.4.cloned.1.call-done = f32[16,2048]{1,0:T(8,128)} async-done(((f32[256,2048]{1,0:T(8,128)}), f32[16,2048]{1,0:T(8,128)}) %reduce-scatter.4.cloned.1.call-update) | async-done | bytes 131088 | tf_op jit(solution)/shard_map/reduce_scatter | solution.py:80
  132.0 1.6 add_divide_fusion
  133.7 58.5 %all-gather.11.cloned.1.call-done = f32[256,2048]{1,0:T(8,128)} async-done(((f32[16,2048]{1,0:T(8,128)}), f32[256,2048]{1,0:T(8,128)}) %all-gather.11.cloned.1.call-update) | async-done | bytes 2097168 | tf_op jit(solution)/shard_map/all_gather | solution.py:86
  192.2 3.3 fusion.37
  195.6 2.2 fusion.36
  197.8 0.7 fusion.35
  198.5 0.7 fusion.34
  199.1 70.9 %all-gather.15.cloned.1.call-done = bf16[16384,128]{1,0:T(8,128)(2,1)} async-done(((bf16[1024,128]{1,0:T(8,128)(2,1)}), bf16[16384,128]{1,0:T(8,128)(2,1)}) %all-gather.15.cloned.1.call-update) | async-done | bytes 4194320 | tf_op jit(solution)/shard_map/all_gather | solution.py:9
  270.0 5.4 %copy.62 = bf16[16,128,8,128]{3,2,0,1:T(8,128)(2,1)} copy(bf16[16,128,8,128]{3,2,1,0:T(8,128)(2,1)} %bitcast.36) | data formatting | bytes 8388608 | tf_op jit(solution)/shard_map/reshape | solution.py:10
  275.4 72.0 %all-gather.13.cloned.1.call-done = bf16[2048,1024]{1,0:T(8,128)(2,1)} async-done(((bf16[128,1024]{1,0:T(8,128)(2,1)}), bf16[2048,1024]{1,0:T(8,128)(2,1)}) %all-gather.13.cloned.1.call-update) | async-done | bytes 4194320 | tf_op jit(solution)/shard_map/all_gather | solution.py:102
  347.5 4.7 %copy.64 = bf16[2048,1024]{1,0:T(8,128)(2,1)} copy(bf16[2048,1024]{1,0:T(8,128)(2,1)} %all-gather.13.cloned.1.call-done) | data formatting | bytes 8388608
  (50 shorter events, 2.7 us)
Async XLA Ops:
  7.2 29.0 %copy-start = (bf16[512,1024]{1,0:T(8,128)(2,1)S(1)}, bf16[512,1024]{1,0:T(8,128)(2,1)}, u32[]{:S(2)}) copy-start(bf16[512,1024]{1,0:T(8,128)(2,1)} %param.16) | copy-start | bytes 3145732
  7.2 1.5 copy-start.3
  7.2 15.7 %all-gather.9.cloned.1.call-start = ((), (), s32[]{:S(2)}) async-start(), calls=%async_computation.2 | async-start | bytes 3145728 | tf_op jit(solution)/shard_map/all_gather | solution.py:60
  7.9 28.3 %all-gather.7.cloned.1.call-start = ((), (), s32[]{:S(2)}) async-start(), calls=%async_computation.1 | async-start | bytes 3145728 | tf_op jit(solution)/shard_map/all_gather | solution.py:59
  8.7 123.3 %reduce-scatter.4.cloned.1.call-start = ((), (), s32[]{:S(2)}) async-start(), calls=%async_computation.6 | async-start | bytes 2228224 | tf_op jit(solution)/shard_map/reduce_scatter | solution.py:80
  9.0 1.2 copy-start.2
  10.5 0.7 copy-start.14
  11.4 0.9 copy-start.15
  22.9 1.6 copy-start.4
  24.5 2.8 copy-start.6
  31.4 8.9 %copy-start.7 = (bf16[2048,256]{1,0:T(8,128)(2,1)S(1)}, bf16[2048,256]{1,0:T(8,128)(2,1)}, u32[]{:S(2)}) copy-start(bf16[2048,256]{1,0:T(8,128)(2,1)} %param.22) | copy-start | bytes 3145732
  49.1 82.9 %copy-start.10 = (f32[16,1024]{1,0:T(8,128)S(1)}, f32[16,1024]{1,0:T(8,128)}, u32[]{:S(2)}) copy-start(f32[16,1024]{1,0:T(8,128)} %param.29) | copy-start | bytes 196612
  49.1 82.9 %copy-start.11 = (f32[16,1024]{1,0:T(8,128)S(1)}, f32[16,1024]{1,0:T(8,128)}, u32[]{:S(2)}) copy-start(f32[16,1024]{1,0:T(8,128)} %param.27) | copy-start | bytes 196612
  49.1 82.9 %copy-start.12 = (f32[16,1024]{1,0:T(8,128)S(1)}, f32[16,1024]{1,0:T(8,128)}, u32[]{:S(2)}) copy-start(f32[16,1024]{1,0:T(8,128)} %param.28) | copy-start | bytes 196612
  49.1 82.9 %copy-start.13 = (f32[16,1024]{1,0:T(8,128)S(1)}, f32[16,1024]{1,0:T(8,128)}, u32[]{:S(2)}) copy-start(f32[16,1024]{1,0:T(8,128)} %param.26) | copy-start | bytes 196612
  49.2 143.0 %copy-start.8 = (f32[1024,128]{1,0:T(8,128)S(1)}, f32[1024,128]{1,0:T(8,128)}, u32[]{:S(2)}) copy-start(f32[1024,128]{1,0:T(8,128)} %param.25) | copy-start | bytes 1572868
  49.2 146.3 %copy-start.9 = (f32[128,1024]{1,0:T(8,128)S(1)}, f32[128,1024]{1,0:T(8,128)}, u32[]{:S(2)}) copy-start(f32[128,1024]{1,0:T(8,128)} %param.24) | copy-start | bytes 1572868
  49.2 143.0 %all-gather.11.cloned.1.call-start = ((), (), s32[]{:S(2)}) async-start(), calls=%async_computation.3 | async-start | bytes 2228224 | tf_op jit(solution)/shard_map/all_gather | solution.py:86
  133.7 136.4 %all-gather.15.cloned.1.call-start = ((), (), s32[]{:S(2)}) async-start(), calls=%async_computation.5 | async-start | bytes 4456448 | tf_op jit(solution)/shard_map/all_gather | solution.py:9
  192.2 3.4 copy-start.5
  195.5 152.0 %all-gather.13.cloned.1.call-start = ((), (), s32[]{:S(2)}) async-start(), calls=%async_computation.4 | async-start | bytes 4456448 | tf_op jit(solution)/shard_map/all_gather | solution.py:102
  347.5 4.7 %copy-start.1 = (bf16[512,1024]{1,0:T(8,128)(2,1)S(1)}, bf16[512,1024]{1,0:T(8,128)(2,1)}, u32[]{:S(2)}) copy-start(bf16[512,1024]{1,0:T(8,128)(2,1)} %param.16) | copy-start | bytes 3145732
Sparse Core Ops, SparseCore 0:
  9.5 13.2 all-gather.8
  24.4 11.7 all-gather.6
  49.3 82.6 reduce-scatter.3
  135.2 56.9 all-gather.10
  195.6 74.3 all-gather.14
  273.2 74.1 all-gather.12
